TPU v7x, 32 devices: a whole 2x2x4 slice. The times are simulated.
32 devices in a mesh: ep: 8 (over z, x), tp: 4 (over y, core).
Axes of the slice: x: 2, y: 2, z: 4, core: 2. Of those that a mesh axis runs over, the one named last changes fastest.
Arguments:
- tokens: bfloat16 [192, 3072], P('ep'), may hold values from -6 to 6
- norm_gain: float32 [3072], replicated, may hold values from 0.1 to 1.9
- routing: int32 [192, 4], P('ep'), may hold values from 0 to 7, all different within a row; in each aligned block of 24 rows (0 to 23, 24 to 47, ...) at most 13 rows name the same one
- route_weight: float32 [192, 4], P('ep'), may hold values from 0.05 to 1
- w_gate: bfloat16 [8, 3072, 3072], P('ep', None, 'tp'), may hold values from -0.3125 to 0.3125
- w_up: bfloat16 [8, 3072, 3072], P('ep', None, 'tp'), may hold values from -0.3125 to 0.3125
- w_down: bfloat16 [8, 3072, 3072], P('ep', 'tp'), may hold values from -0.01953125 to 0.01953125
Outputs:
- mixed: bfloat16 [192, 3072], P('ep', 'tp')
Inputs may be any that keep to these rules, and one draw needn't show every extreme that they name: `routing`: each row names 4 different experts. Within the rows of one device (aligned blocks of 24 rows) no expert is named by more than 13 rows, a bound that some block reaches.
All inputs are finite; a program needn't handle non-finite values.
Results may differ from a plain program's by a relative error of at most 0.019.
Values may be sent and summed in bfloat16 or wider, within the bound.
No kernel may reach another device: no remote copies, remote signals or barrier semaphores. Data moves between devices by JAX's collectives and lax.ppermute only.
A program may use at most 64 MiB of HBM per device.

v0:
```python
import jax
import jax.numpy as jnp
from jax import lax
from jax.sharding import PartitionSpec as P

NORM_EPS = 1e-06
CLAMP_LIMIT = 7.0
SIGMOID_SCALE = 1.702


def slot_index(route_rows, expert_total, capacity):
    flat_ids = route_rows.reshape(-1)
    one_hot = (flat_ids[:, None] == jnp.arange(expert_total, dtype=jnp.int32)[None, :]).astype(
        jnp.int32
    )
    before = jnp.cumsum(one_hot, axis=0) - one_hot
    ranked = jnp.sum(before * one_hot, axis=1)
    return flat_ids * capacity + ranked


def local(tokens, norm_gain, routing, route_weight, w_gate, w_up, w_down):
    tok_count = tokens.shape[0]
    width = tokens.shape[1]
    top_count = routing.shape[1]
    expert_total = lax.axis_size("ep") * w_gate.shape[0]
    capacity = max(2, tok_count * top_count // expert_total + 1)
    slice_width = width // lax.axis_size("tp")
    values = tokens.astype(jnp.float32)
    scaled = values * lax.rsqrt(jnp.mean(values * values, axis=-1, keepdims=True) + NORM_EPS)
    normal = (scaled * norm_gain).astype(jnp.bfloat16)
    dest = slot_index(routing, expert_total, capacity)
    slot_ids = jnp.arange(expert_total * capacity, dtype=jnp.int32)
    select = jnp.sum(dest.reshape(1, tok_count, top_count) == slot_ids[:, None, None], axis=2)
    sending = jnp.dot(
        select.astype(jnp.bfloat16), normal, preferred_element_type=jnp.float32
    ).astype(jnp.bfloat16)
    gate_mat = w_gate[0]
    up_mat = w_up[0]
    down_mat = w_down[0]
    own_share = lax.dynamic_slice_in_dim(
        sending, lax.axis_index("tp") * slice_width, slice_width, 1
    )
    arrived = lax.all_to_all(own_share, "ep", split_axis=0, concat_axis=0, tiled=True)
    pieces = lax.all_gather(arrived, "tp", axis=1, tiled=True)
    gate_pre = jnp.dot(pieces, gate_mat, preferred_element_type=jnp.float32)
    up_pre = jnp.dot(pieces, up_mat, preferred_element_type=jnp.float32)
    gated = jnp.minimum(gate_pre, CLAMP_LIMIT)
    upper = jnp.clip(up_pre, -CLAMP_LIMIT, CLAMP_LIMIT)
    hidden = ((upper + 1.0) * gated * jax.nn.sigmoid(SIGMOID_SCALE * gated)).astype(jnp.bfloat16)
    summed = lax.psum_scatter(
        lax.dot_general(
            down_mat, hidden, (((0,), (1,)), ((), ())), preferred_element_type=jnp.float32
        ).astype(jnp.bfloat16),
        "tp",
        scatter_dimension=0,
        tiled=True,
    )
    back = lax.all_to_all(summed, "ep", split_axis=1, concat_axis=1, tiled=True)
    picked = back[:, dest].reshape(slice_width, tok_count, top_count)
    mixed = jnp.sum(picked.astype(jnp.float32) * route_weight[None, :, :], axis=2)
    return mixed.T.astype(jnp.bfloat16)


def solution(mesh):
    placed = (
        P("ep", None),
        P(),
        P("ep", None),
        P("ep", None),
        P("ep", None, "tp"),
        P("ep", None, "tp"),
        P("ep", "tp", None),
    )
    return jax.shard_map(
        local, mesh=mesh, in_specs=placed, out_specs=P("ep", "tp"), check_vma=False
    )
```

profile of v0, /device:TPU:0, one launch (start us, length us, event | category | flops | bytes accessed | tf_op | source)
XLA Modules:
  0.0 87.3 jit_solution(828306079801427838)
XLA Ops:
  6.5 0.8 copy.14
  7.3 0.1 eq.28
  7.4 0.1 fusion.48
  7.5 0.1 reduce_window_sum.11
  7.6 0.2 select_reduce_fusion
  7.8 0.1 reduce_sum.41
  7.9 0.1 copy.16
  8.0 0.1 convert_reduce_fusion
  8.1 1.0 %fusion.37 = f32[24]{0:T(128)S(1)} fusion(bf16[24,3072]{1,0:T(8,128)(2,1)} %param.7), kind=kLoop, calls=%fused_computation.23 | loop fusion | flops 221160 | bytes 147552 | tf_op jit(solution)/shard_map/reduce_sum | solution.py:29
  9.2 1.3 %fusion.44 = bf16[104,3072]{1,0:T(8,128)(2,1)S(1)} fusion(bf16[24,3072]{1,0:T(8,128)(2,1)} %param.7, f32[3072]{0:T(1024)} %param.8, f32[24]{0:T(128)S(1)} %add_rsqrt_fusion, s32[104,24]{0,1:T(8,128)S(1)} %convert_reduce_fusion), kind=kOutput, calls=%fused_computation.32 | convolution fusion | flops 15632832 | bytes 808800 | tf_op jit(solution)/shard_map/dot_general | solution.py:34
  10.6 15.0 %all_to_all.24 = bf16[8,13,768]{2,1,0:T(8,128)(2,1)S(1)} all-to-all(bf16[8,13,768]{2,1,0:T(8,128)(2,1)S(1)} %all_to_all.16), channel_id=1, replica_groups=mesh['ep'=8,'tp'=4] {'ep'}, dimensions={0} | all-to-all | bytes 319488 | tf_op jit(solution)/shard_map/all_to_all | solution.py:43
  25.6 0.1 all_to_all.18
  25.7 7.8 %all_gather.3 = bf16[104,3072]{1,0:T(8,128)(2,1)S(1)} all-gather(bf16[104,768]{1,0:T(8,128)(2,1)S(1)} %all_to_all.18), channel_id=1, replica_groups=mesh['ep'=8,'tp'=4] {'tp'}, dimensions={1}, use_global_device_ids=true | all-gather | bytes 798720 | tf_op jit(solution)/shard_map/all_gather | solution.py:44
  33.5 3.2 %fusion.12 = f32[104,768]{1,0:T(8,128)S(1)} fusion(bf16[104,3072]{1,0:T(8,128)(2,1)S(1)} %all_gather.3, bf16[1,3072,768]{2,1,0:T(8,128)(2,1)} %param.11), kind=kOutput, calls=%fused_computation.9 | convolution fusion | flops 490813440 | bytes 5677056 | tf_op jit(solution)/shard_map/dot_general | solution.py:45
  36.7 6.5 %fusion.9 = bf16[3072,104]{0,1:T(8,128)(2,1)} fusion(bf16[1,768,3072]{2,1,0:T(8,128)(2,1)} %param.13, f32[104,768]{1,0:T(8,128)S(1)} %fusion.12, bf16[104,3072]{1,0:T(8,128)(2,1)S(1)} %all_gather.3, bf16[1,3072,768]{2,1,0:T(8,128)(2,1)} %param.12), kind=kOutput, calls=%fused_computation.8 | convolution fusion | flops 982505472 | bytes 11034624 | tf_op jit(solution)/shard_map/dot_general | solution.py:51
  43.2 0.1 mul.76
  43.4 0.1 copy.17
  43.4 20.2 %reduce-scatter.2.cloned.1.call-done = bf16[768,104]{0,1:T(8,128)(2,1)} async-done(((bf16[3072,104]{0,1:T(8,128)(2,1)}), bf16[768,104]{0,1:T(8,128)(2,1)}) %reduce-scatter.2.cloned.1.call-update) | async-done | bytes 159760 | tf_op jit(solution)/shard_map/reduce_scatter | solution.py:50
  63.7 1.6 %all_to_all.19 = bf16[768,8,13]{0,2,1:T(8,128)(2,1)} reshape(bf16[768,104]{0,1:T(8,128)(2,1)} %reduce-scatter.2.cloned.1.call-done) | data formatting | bytes 319488 | tf_op jit(solution)/shard_map/all_to_all | solution.py:58
  65.3 5.5 %all-to-all-start.1 = ((bf16[768,8,13]{0,2,1:T(8,128)(2,1)}), bf16[768,8,13]{0,2,1:T(8,128)(2,1)S(1)}, u32[]{:S(2)}, u32[]{:S(2)}) async-start(bf16[768,8,13]{0,2,1:T(8,128)(2,1)} %all_to_all.19), calls=%async_computation.2 | async-start | bytes 393216 | tf_op jit(solution)/shard_map/all_to_all | solution.py:58
  70.8 7.8 %all-to-all-done.1 = bf16[768,8,13]{0,2,1:T(8,128)(2,1)S(1)} async-done(((bf16[768,8,13]{0,2,1:T(8,128)(2,1)}), bf16[768,8,13]{0,2,1:T(8,128)(2,1)S(1)}, u32[]{:S(2)}, u32[]{:S(2)}) %all-to-all-start.1) | async-done | bytes 159776 | tf_op jit(solution)/shard_map/all_to_all | solution.py:58
  78.7 0.8 gather_fusion
  79.5 0.1 reshape.54
  79.6 0.9 multiply_reduce_fusion
  (12 shorter events, 0.2 us)
Async XLA Ops:
  6.5 57.1 %reduce-scatter.2.cloned.1.call-start = ((), (), s32[]{:S(2)}) async-start(), calls=%async_computation.3 | async-start | bytes 798720 | tf_op jit(solution)/shard_map/reduce_scatter | solution.py:50
  36.7 6.7 %copy-start = (f32[24,4]{0,1:T(4,128)S(1)}, f32[24,4]{0,1:T(4,128)}, u32[]{:S(2)}) copy-start(f32[24,4]{0,1:T(4,128)} %param.10) | copy-start | bytes 1156
  65.3 13.3 %all-to-all-start.1 = ((bf16[768,8,13]{0,2,1:T(8,128)(2,1)}), bf16[768,8,13]{0,2,1:T(8,128)(2,1)S(1)}, u32[]{:S(2)}, u32[]{:S(2)}) async-start(bf16[768,8,13]{0,2,1:T(8,128)(2,1)} %all_to_all.19), calls=%async_computation.2 | async-start | bytes 393216 | tf_op jit(solution)/shard_map/all_to_all | solution.py:58
Sparse Core Ops, SparseCore 0:
  43.4 20.2 reduce-scatter.1
where the time goes:
time: 87.7 us; the launch traced here: 87.3 us
  waiting for transfers between devices  28 us (32%)
  blocking collectives  22.9 us (26%)
  between operations  13.5 us (15%)
  matrix products  11 us (13%)
  starting transfers between devices  5.5 us (6%)
  local copies, waits for them, and re-layouts  3.96 us (5%)
  other arithmetic  2.44 us (3%)
    reduce_scatter x1, waiting for transfers between devices, local(): lax.psum_scatter(lax.dot_general(down_mat, hidden, (((0,), (1,)), ((), ()...  20.2 us
    all_to_all x1, blocking collectives, local(): lax.all_to_all(own_share, 'ep', split_axis=0, concat_axis=0, tiled=True)  15 us
    all_gather x1, blocking collectives, local(): pieces = lax.all_gather(arrived, 'tp', axis=1, tiled=True)  7.82 us
    all_to_all x1, waiting for transfers between devices, local(): back = lax.all_to_all(summed, 'ep', split_axis=1, concat_axis=1, tiled=True)  7.77 us
    dot_general x1, matrix products, local(): lax.dot_general(down_mat, hidden, (((0,), (1,)), ((), ())), preferred_ele...  6.54 us
    all_to_all x1, starting transfers between devices, local(): back = lax.all_to_all(summed, 'ep', split_axis=1, concat_axis=1, tiled=True)  5.5 us
    dot_general x1, matrix products, local(): gate_pre = jnp.dot(pieces, gate_mat, preferred_element_type=jnp.float32)  3.18 us
  transfers between devices with their start and end apart: 2, of which 2 were waited for; matrix products, arithmetic and copies ran while one was open for 0% of the time, Pallas kernels for 0%

commit v1 on v0

--- a/solution.py
+++ b/solution.py
@@ -41,7 +41,7 @@
         sending, lax.axis_index("tp") * slice_width, slice_width, 1
     )
     arrived = lax.all_to_all(own_share, "ep", split_axis=0, concat_axis=0, tiled=True)
-    pieces = lax.all_gather(arrived, "tp", axis=1, tiled=True)
+    pieces = jnp.concatenate(lax.all_gather(arrived, "tp"), axis=1)
     gate_pre = jnp.dot(pieces, gate_mat, preferred_element_type=jnp.float32)
     up_pre = jnp.dot(pieces, up_mat, preferred_element_type=jnp.float32)
     gated = jnp.minimum(gate_pre, CLAMP_LIMIT)

time: 87.7 us -> 87.7 us (level)
  no operation moved by 1% of the time
where the time goes in v1:
time: 87.7 us; the launch traced here: 87.4 us
  waiting for transfers between devices  28 us (32%)
  blocking collectives  22.9 us (26%)
  between operations  13.5 us (15%)
  matrix products  11 us (13%)
  starting transfers between devices  5.53 us (6%)
  local copies, waits for them, and re-layouts  4.02 us (5%)
  other arithmetic  2.44 us (3%)
    reduce_scatter x1, waiting for transfers between devices, local(): lax.psum_scatter(lax.dot_general(down_mat, hidden, (((0,), (1,)), ((), ()...  20.2 us
    all_to_all x1, blocking collectives, local(): lax.all_to_all(own_share, 'ep', split_axis=0, concat_axis=0, tiled=True)  15 us
    all_gather x1, blocking collectives, local(): pieces = jnp.concatenate(lax.all_gather(arrived, 'tp'), axis=1)  7.82 us
    all_to_all x1, waiting for transfers between devices, local(): back = lax.all_to_all(summed, 'ep', split_axis=1, concat_axis=1, tiled=True)  7.77 us
    dot_general x1, matrix products, local(): lax.dot_general(down_mat, hidden, (((0,), (1,)), ((), ())), preferred_ele...  6.54 us
    all_to_all x1, starting transfers between devices, local(): back = lax.all_to_all(summed, 'ep', split_axis=1, concat_axis=1, tiled=True)  5.52 us
    dot_general x1, matrix products, local(): gate_pre = jnp.dot(pieces, gate_mat, preferred_element_type=jnp.float32)  3.18 us
  transfers between devices with their start and end apart: 2, of which 2 were waited for; matrix products, arithmetic and copies ran while one was open for 0% of the time, Pallas kernels for 0%

profile of v1, /device:TPU:0, one launch (start us, length us, event | category | flops | bytes accessed | tf_op | source)
XLA Modules:
  0.0 87.4 jit_solution(16225843954624104547)
XLA Ops:
  6.5 0.8 copy.19
  7.3 0.1 eq.28
  7.4 0.1 fusion.48
  7.5 0.1 reduce_window_sum.11
  7.6 0.2 select_reduce_fusion
  7.8 0.1 reduce_sum.41
  7.9 0.1 copy.21
  8.0 0.1 convert_reduce_fusion
  8.1 1.0 %fusion.37 = f32[24]{0:T(128)S(1)} fusion(bf16[24,3072]{1,0:T(8,128)(2,1)} %param.7), kind=kLoop, calls=%fused_computation.23 | loop fusion | flops 221160 | bytes 147552 | tf_op jit(solution)/shard_map/reduce_sum | solution.py:29
  9.2 1.3 %fusion.44 = bf16[104,3072]{1,0:T(8,128)(2,1)S(1)} fusion(bf16[24,3072]{1,0:T(8,128)(2,1)} %param.7, f32[3072]{0:T(1024)} %param.8, f32[24]{0:T(128)S(1)} %add_rsqrt_fusion, s32[104,24]{0,1:T(8,128)S(1)} %convert_reduce_fusion), kind=kOutput, calls=%fused_computation.32 | convolution fusion | flops 15632832 | bytes 808800 | tf_op jit(solution)/shard_map/dot_general | solution.py:34
  10.6 15.0 %all_to_all.21 = bf16[8,13,768]{2,1,0:T(8,128)(2,1)S(1)} all-to-all(bf16[8,13,768]{2,1,0:T(8,128)(2,1)S(1)} %all_to_all.14), channel_id=1, replica_groups=mesh['ep'=8,'tp'=4] {'ep'}, dimensions={0} | all-to-all | bytes 319488 | tf_op jit(solution)/shard_map/all_to_all | solution.py:43
  25.6 0.1 all_gather.6
  25.7 7.8 %all_gather.7 = bf16[4,104,768]{2,1,0:T(8,128)(2,1)S(1)} all-gather(bf16[1,104,768]{2,1,0:T(8,128)(2,1)S(1)} %all_gather.6), channel_id=1, replica_groups=mesh['ep'=8,'tp'=4] {'tp'}, dimensions={0}, use_global_device_ids=true | all-gather | bytes 798720 | tf_op jit(solution)/shard_map/all_gather | solution.py:44
  33.6 3.2 %fusion.12 = f32[104,768]{1,0:T(8,128)S(1)} fusion(bf16[104,3072]{1,0:T(8,128)(2,1)S(1)} %bitcast.51, bf16[1,3072,768]{2,1,0:T(8,128)(2,1)} %param.11), kind=kOutput, calls=%fused_computation.9 | convolution fusion | flops 490813440 | bytes 5677056 | tf_op jit(solution)/shard_map/dot_general | solution.py:45
  36.7 6.5 %fusion.9 = bf16[3072,104]{0,1:T(8,128)(2,1)} fusion(bf16[1,768,3072]{2,1,0:T(8,128)(2,1)} %param.13, f32[104,768]{1,0:T(8,128)S(1)} %fusion.12, bf16[104,3072]{1,0:T(8,128)(2,1)S(1)} %bitcast.52, bf16[1,3072,768]{2,1,0:T(8,128)(2,1)} %param.12), kind=kOutput, calls=%fused_computation.8 | convolution fusion | flops 982505472 | bytes 11034624 | tf_op jit(solution)/shard_map/dot_general | solution.py:51
  43.3 0.1 mul.76
  43.4 0.1 copy.23
  43.5 20.2 %reduce-scatter.2.cloned.1.call-done = bf16[768,104]{0,1:T(8,128)(2,1)} async-done(((bf16[3072,104]{0,1:T(8,128)(2,1)}), bf16[768,104]{0,1:T(8,128)(2,1)}) %reduce-scatter.2.cloned.1.call-update) | async-done | bytes 159760 | tf_op jit(solution)/shard_map/reduce_scatter | solution.py:50
  63.7 1.6 %all_to_all.16 = bf16[768,8,13]{0,2,1:T(8,128)(2,1)} reshape(bf16[768,104]{0,1:T(8,128)(2,1)} %reduce-scatter.2.cloned.1.call-done) | data formatting | bytes 319488 | tf_op jit(solution)/shard_map/all_to_all | solution.py:58
  65.4 5.5 %all-to-all-start.1 = ((bf16[768,8,13]{0,2,1:T(8,128)(2,1)}), bf16[768,8,13]{0,2,1:T(8,128)(2,1)S(1)}, u32[]{:S(2)}, u32[]{:S(2)}) async-start(bf16[768,8,13]{0,2,1:T(8,128)(2,1)} %all_to_all.16), calls=%async_computation.2 | async-start | bytes 393216 | tf_op jit(solution)/shard_map/all_to_all | solution.py:58
  70.9 7.8 %all-to-all-done.1 = bf16[768,8,13]{0,2,1:T(8,128)(2,1)S(1)} async-done(((bf16[768,8,13]{0,2,1:T(8,128)(2,1)}), bf16[768,8,13]{0,2,1:T(8,128)(2,1)S(1)}, u32[]{:S(2)}, u32[]{:S(2)}) %all-to-all-start.1) | async-done | bytes 159776 | tf_op jit(solution)/shard_map/all_to_all | solution.py:58
  78.8 0.8 gather_fusion
  79.6 0.1 reshape.63
  79.7 0.9 multiply_reduce_fusion
  (13 shorter events, 0.3 us)
Async XLA Ops:
  6.5 57.2 %reduce-scatter.2.cloned.1.call-start = ((), (), s32[]{:S(2)}) async-start(), calls=%async_computation.3 | async-start | bytes 798720 | tf_op jit(solution)/shard_map/reduce_scatter | solution.py:50
  36.7 6.7 %copy-start = (f32[24,4]{0,1:T(4,128)S(1)}, f32[24,4]{0,1:T(4,128)}, u32[]{:S(2)}) copy-start(f32[24,4]{0,1:T(4,128)} %param.10) | copy-start | bytes 1156
  65.4 13.3 %all-to-all-start.1 = ((bf16[768,8,13]{0,2,1:T(8,128)(2,1)}), bf16[768,8,13]{0,2,1:T(8,128)(2,1)S(1)}, u32[]{:S(2)}, u32[]{:S(2)}) async-start(bf16[768,8,13]{0,2,1:T(8,128)(2,1)} %all_to_all.16), calls=%async_computation.2 | async-start | bytes 393216 | tf_op jit(solution)/shard_map/all_to_all | solution.py:58
Sparse Core Ops, SparseCore 0:
  43.4 20.2 reduce-scatter.1
